TPU v7x, 32 devices: a whole 2x2x4 slice. The times are simulated.
32 devices in a mesh: fs: 4 (over z), rep: 4 (over y, x), tp: 2 (over core).
Axes of the slice: x: 2, y: 2, z: 4, core: 2. Of those that a mesh axis runs over, the one named last changes fastest.
Arguments:
- normed_input: bfloat16 [4096, 2048], P(('fs', 'rep')), may hold values from -20 to 20
- key_cotangent: bfloat16 [4096, 2048], P(('fs', 'rep'), 'tp'), may hold values from -0.03125 to 0.03125
- value_cotangent: bfloat16 [4096, 4096], P(('fs', 'rep'), 'tp'), may hold values from -0.03125 to 0.03125
- key_basis: bfloat16 [2048, 256], P('tp'), may hold values from -0.375 to 0.375
- value_basis: bfloat16 [4096, 256], P('tp'), may hold values from -0.375 to 0.375
- key_master: float32 [2048, 2048], P('fs', 'tp'), may hold values from -0.125 to 0.125
- value_master: float32 [2048, 4096], P('fs', 'tp'), may hold values from -0.125 to 0.125
- key_moment: float32 [2048, 256], P(('fs', 'rep'), 'tp'), may hold values from -200 to 200
- key_second: float32 [2048, 256], P(('fs', 'rep'), 'tp'), may hold values from 0.05 to 0.5
- value_moment: float32 [2048, 256], P(('fs', 'rep'), 'tp'), may hold values from -200 to 200
- value_second: float32 [2048, 256], P(('fs', 'rep'), 'tp'), may hold values from 0.05 to 0.5
Outputs:
- key_mean: float32 [2048, 256], P(('fs', 'rep'), 'tp')
- key_square: float32 [2048, 256], P(('fs', 'rep'), 'tp')
- value_mean: float32 [2048, 256], P(('fs', 'rep'), 'tp')
- value_square: float32 [2048, 256], P(('fs', 'rep'), 'tp')
- key_step: float32 [2048, 2048], P('fs', 'tp')
- value_step: float32 [2048, 4096], P('fs', 'tp')
- key_weight: bfloat16 [2048, 2048], P('fs', 'tp')
- value_weight: bfloat16 [2048, 4096], P('fs', 'tp')
All inputs are finite; a program needn't handle non-finite values.
Results may differ from a plain program's by a relative error of at most 0.0034.
Values may be sent and summed in bfloat16 or wider, within the bound.
A program may use at most 64 MiB of HBM per device.

v0:
```python
import jax
import jax.numpy as jnp
from jax import lax
from jax.sharding import PartitionSpec as P

D = 2048
RANK = 256


first_decay = 0.8
second_decay = 0.9
root_epsilon = 1e-08
mean_epsilon = 1e-06
learn_rate = 0.01


def shards(
    normed_input,
    key_cotangent,
    value_cotangent,
    key_basis,
    value_basis,
    key_master,
    value_master,
    key_moment,
    key_second,
    value_moment,
    value_second,
):
    key_proj = jnp.dot(key_cotangent, key_basis, preferred_element_type=jnp.float32)
    value_proj = jnp.dot(value_cotangent, value_basis, preferred_element_type=jnp.float32)
    width = key_moment.shape[1]
    key_part, value_part = (
        lax.psum_scatter(key_proj, "tp", scatter_dimension=1, tiled=True),
        lax.psum_scatter(value_proj, "tp", scatter_dimension=1, tiled=True),
    )
    joined = jnp.concatenate(
        [key_part.astype(jnp.bfloat16), value_part.astype(jnp.bfloat16)], axis=1
    )
    summed = lax.psum_scatter(
        lax.dot_general(
            normed_input, joined, (((0,), (0,)), ((), ())), preferred_element_type=jnp.float32
        ),
        ("fs", "rep"),
        scatter_dimension=0,
        tiled=True,
    )
    key_grad = summed[:, :width]
    value_grad = summed[:, width:]
    key_mean = first_decay * key_moment + (1.0 - first_decay) * key_grad
    value_mean = first_decay * value_moment + (1.0 - first_decay) * value_grad
    key_square = second_decay * key_second + (1.0 - second_decay) * key_grad * key_grad
    value_square = second_decay * value_second + (1.0 - second_decay) * value_grad * value_grad
    key_ratio = key_mean / (jnp.sqrt(key_square) + root_epsilon)
    value_ratio = value_mean / (jnp.sqrt(value_square) + root_epsilon)
    local_total = jnp.sum(key_ratio * key_ratio) + jnp.sum(value_ratio * value_ratio)
    total = lax.psum(local_total, ("fs", "rep", "tp"))
    scale = jnp.sqrt(total / (2 * D * RANK) + mean_epsilon)
    key_dir = (key_ratio / scale).astype(jnp.bfloat16)
    value_dir = (value_ratio / scale).astype(jnp.bfloat16)
    key_dir, value_dir = (
        lax.all_gather(key_dir, "rep", axis=0, tiled=True),
        lax.all_gather(value_dir, "rep", axis=0, tiled=True),
    )
    key_dir, value_dir = (
        lax.all_gather(key_dir, "tp", axis=1, tiled=True),
        lax.all_gather(value_dir, "tp", axis=1, tiled=True),
    )
    dims = (((1,), (1,)), ((), ()))
    key_step = lax.dot_general(key_dir, key_basis, dims, preferred_element_type=jnp.float32)
    value_step = lax.dot_general(value_dir, value_basis, dims, preferred_element_type=jnp.float32)
    key_weight = (key_master - learn_rate * key_step).astype(jnp.bfloat16)
    value_weight = (value_master - learn_rate * value_step).astype(jnp.bfloat16)
    return (
        key_mean,
        key_square,
        value_mean,
        value_square,
        key_step,
        value_step,
        key_weight,
        value_weight,
    )


def solution(mesh):
    placed = (
        P(("fs", "rep"), None),
        P(("fs", "rep"), "tp"),
        P(("fs", "rep"), "tp"),
        P("tp", None),
        P("tp", None),
        P("fs", "tp"),
        P("fs", "tp"),
        P(("fs", "rep"), "tp"),
        P(("fs", "rep"), "tp"),
        P(("fs", "rep"), "tp"),
        P(("fs", "rep"), "tp"),
    )
    return jax.shard_map(
        shards,
        mesh=mesh,
        in_specs=placed,
        out_specs=(
            P(("fs", "rep"), "tp"),
            P(("fs", "rep"), "tp"),
            P(("fs", "rep"), "tp"),
            P(("fs", "rep"), "tp"),
            P("fs", "tp"),
            P("fs", "tp"),
            P("fs", "tp"),
            P("fs", "tp"),
        ),
        check_vma=False,
    )
```

profile of v0, /device:TPU:0, one launch (start us, length us, event | category | flops | bytes accessed | tf_op | source)
XLA Modules:
  0.0 195.8 jit_solution(8148768038539851981)
XLA Ops:
  7.2 0.0 copy-start
  7.2 0.0 copy-start.3
  7.2 0.0 reduce-scatter.4.cloned.1.call-start
  7.2 2.3 %fusion.8 = f32[256,256]{1,0:T(8,128)} fusion(bf16[256,1024]{1,0:T(8,128)(2,1)} %param.12, bf16[1024,256]{1,0:T(8,128)(2,1)} %param.14), kind=kOutput, calls=%fused_computation.19 | convolution fusion | flops 134217728 | bytes 1310720 | tf_op jit(solution)/shard_map/dot_general | solution.py:30
  9.6 0.0 reduce-scatter.4.cloned.1.call-update
  9.6 0.0 reduce-scatter.6.cloned.1.call-start
  9.7 0.0 copy-done
  9.7 2.4 %fusion.9 = f32[256,256]{1,0:T(8,128)} fusion(bf16[256,2048]{1,0:T(8,128)(2,1)} %param.13, bf16[2048,256]{1,0:T(8,128)(2,1)S(1)} %copy-done), kind=kOutput, calls=%fused_computation.20 | convolution fusion | flops 268435456 | bytes 2359296 | tf_op jit(solution)/shard_map/dot_general | solution.py:31
  12.0 0.0 reduce-scatter.6.cloned.1.call-update
  12.1 0.0 reduce-scatter.8.cloned.1.call-start
  12.1 9.2 %reduce-scatter.4.cloned.1.call-done = f32[256,128]{1,0:T(8,128)} async-done(((f32[256,256]{1,0:T(8,128)}), f32[256,128]{1,0:T(8,128)}) %reduce-scatter.4.cloned.1.call-update) | async-done | bytes 131088 | tf_op jit(solution)/shard_map/reduce_scatter | solution.py:34
  21.3 0.9 convert_element_type.18
  22.2 10.8 %reduce-scatter.6.cloned.1.call-done = f32[256,128]{1,0:T(8,128)} async-done(((f32[256,256]{1,0:T(8,128)}), f32[256,128]{1,0:T(8,128)}) %reduce-scatter.6.cloned.1.call-update) | async-done | bytes 131088 | tf_op jit(solution)/shard_map/reduce_scatter | solution.py:35
  33.0 0.9 convert_element_type.19
  33.9 0.0 copy-done.3
  33.9 0.0 copy-start.4
  33.9 0.0 copy-start.5
  33.9 0.0 copy-start.6
  33.9 0.0 copy-start.7
  33.9 1.8 convolution_bitcast_fusion
  35.7 0.0 reduce-scatter.8.cloned.1.call-update
  35.7 0.0 copy-done.4
  35.8 0.0 copy-start.2
  35.8 0.1 copy.19
  35.9 0.0 copy-done.5
  35.9 0.1 copy.20
  36.0 0.0 copy-done.6
  36.0 0.7 copy.21
  36.7 0.0 copy-done.7
  36.7 0.7 copy.22
  37.4 81.1 %reduce-scatter.8.cloned.1.call-done = f32[128,256]{0,1:T(8,128)} async-done(((f32[2048,256]{0,1:T(8,128)}), f32[128,256]{0,1:T(8,128)}) %reduce-scatter.8.cloned.1.call-update) | async-done | bytes 131088 | tf_op jit(solution)/shard_map/reduce_scatter | solution.py:40
  118.6 1.6 multiply_reduce_fusion
  121.5 36.8 %psum.7 = f32[]{:T(128)} all-reduce(f32[]{:T(128)S(6)} %add.38), channel_id=1, replica_groups=mesh['fs'=4,'rep'=4,'tp'=2] {'fs','rep','tp'}, use_global_device_ids=true, to_apply=%region_5.0 | all-reduce | flops 1 | bytes 8 | tf_op jit(solution)/shard_map/psum | solution.py:57
  159.0 0.7 copy.26
  159.8 0.7 copy.25
  160.5 0.7 copy.24
  161.3 0.7 copy.23
  162.0 9.4 %all_gather.12 = bf16[512,128]{0,1:T(8,128)(2,1)S(1)} all-gather(bf16[128,128]{0,1:T(8,128)(2,1)S(1)} %divide_convert_fusion.1), channel_id=1, replica_groups=mesh['fs'=4,'rep'=4,'tp'=2] {'rep'}, dimensions={0}, use_global_device_ids=true | all-gather | bytes 163840 | tf_op jit(solution)/shard_map/all_gather | solution.py:62
  171.4 7.0 %all_gather.14 = bf16[512,128]{0,1:T(8,128)(2,1)S(1)} all-gather(bf16[128,128]{0,1:T(8,128)(2,1)S(1)} %divide_convert_fusion), channel_id=1, replica_groups=mesh['fs'=4,'rep'=4,'tp'=2] {'rep'}, dimensions={0}, use_global_device_ids=true | all-gather | bytes 163840 | tf_op jit(solution)/shard_map/all_gather | solution.py:63
  178.5 2.0 %all_gather.15 = bf16[512,256]{0,1:T(8,128)(2,1)S(1)} all-gather(bf16[512,128]{0,1:T(8,128)(2,1)S(1)} %all_gather.14), channel_id=1, replica_groups=mesh['fs'=4,'rep'=4,'tp'=2] {'tp'}, dimensions={1}, use_global_device_ids=true | all-gather | bytes 393216 | tf_op jit(solution)/shard_map/all_gather | solution.py:67
  180.5 2.0 %all_gather.13 = bf16[512,256]{0,1:T(8,128)(2,1)S(1)} all-gather(bf16[512,128]{0,1:T(8,128)(2,1)S(1)} %all_gather.12), channel_id=1, replica_groups=mesh['fs'=4,'rep'=4,'tp'=2] {'tp'}, dimensions={1}, use_global_device_ids=true | all-gather | bytes 393216 | tf_op jit(solution)/shard_map/all_gather | solution.py:66
  182.4 0.0 copy-done.2
  182.4 0.0 copy-start.1
  182.5 3.4 %subtract_convert_fusion.1 = (bf16[512,1024]{1,0:T(8,128)(2,1)}, f32[512,1024]{1,0:T(8,128)}) fusion(f32[512,1024]{1,0:T(8,128)S(1)} %copy-done.2, bf16[512,256]{0,1:T(8,128)(2,1)S(1)} %all_gather.13, bf16[1024,256]{1,0:T(8,128)(2,1)} %param.14), kind=kOutput, calls=%fused_computation.2 | convolution fusion | flops 270008320 | bytes 6029312 | tf_op jit(solution)/shard_map/dot_general | solution.py:70
  185.8 0.0 copy-done.1
  185.8 3.5 %subtract_convert_fusion = (bf16[512,2048]{1,0:T(8,128)(2,1)}, f32[512,2048]{1,0:T(8,128)}) fusion(f32[512,2048]{1,0:T(8,128)S(1)} %copy-done.1, bf16[512,256]{0,1:T(8,128)(2,1)S(1)} %all_gather.15, bf16[2048,256]{1,0:T(8,128)(2,1)S(1)} %copy-done), kind=kOutput, calls=%fused_computation | convolution fusion | flops 540016640 | bytes 11796480 | tf_op jit(solution)/shard_map/dot_general | solution.py:71
  (2 shorter events, 0.1 us)
Async XLA Ops:
  7.2 2.5 %copy-start = (bf16[2048,256]{1,0:T(8,128)(2,1)S(1)}, bf16[2048,256]{1,0:T(8,128)(2,1)}, u32[]{:S(2)}) copy-start(bf16[2048,256]{1,0:T(8,128)(2,1)} %param.15) | copy-start | bytes 3145732
  7.2 26.7 %copy-start.3 = (bf16[256,2048]{1,0:T(8,128)(2,1)S(1)}, bf16[256,2048]{1,0:T(8,128)(2,1)}, u32[]{:S(2)}) copy-start(bf16[256,2048]{1,0:T(8,128)(2,1)} %param.11) | copy-start | bytes 3145732
  7.2 14.1 %reduce-scatter.4.cloned.1.call-start = ((), (), s32[]{:S(2)}) async-start(), calls=%async_computation.3 | async-start | bytes 393216 | tf_op jit(solution)/shard_map/reduce_scatter | solution.py:34
  9.6 23.4 %reduce-scatter.6.cloned.1.call-start = ((), (), s32[]{:S(2)}) async-start(), calls=%async_computation.4 | async-start | bytes 393216 | tf_op jit(solution)/shard_map/reduce_scatter | solution.py:35
  12.1 106.5 %reduce-scatter.8.cloned.1.call-start = ((), (), s32[]{:S(2)}) async-start(), calls=%async_computation.5 | async-start | bytes 2228224 | tf_op jit(solution)/shard_map/reduce_scatter | solution.py:40
  33.9 1.9 copy-start.4
  33.9 2.0 %copy-start.5 = (f32[128,128]{1,0:T(8,128)S(1)}, f32[128,128]{1,0:T(8,128)}, u32[]{:S(2)}) copy-start(f32[128,128]{1,0:T(8,128)} %param.19) | copy-start | bytes 196612
  33.9 2.1 %copy-start.6 = (f32[128,128]{1,0:T(8,128)S(1)}, f32[128,128]{1,0:T(8,128)}, u32[]{:S(2)}) copy-start(f32[128,128]{1,0:T(8,128)} %param.20) | copy-start | bytes 196612
  33.9 2.8 %copy-start.7 = (f32[128,128]{1,0:T(8,128)S(1)}, f32[128,128]{1,0:T(8,128)}, u32[]{:S(2)}) copy-start(f32[128,128]{1,0:T(8,128)} %param.21) | copy-start | bytes 196612
  35.8 146.7 %copy-start.2 = (f32[512,1024]{1,0:T(8,128)S(1)}, f32[512,1024]{1,0:T(8,128)}, u32[]{:S(2)}) copy-start(f32[512,1024]{1,0:T(8,128)} %param.16) | copy-start | bytes 6291460
  182.4 3.4 %copy-start.1 = (f32[512,2048]{1,0:T(8,128)S(1)}, f32[512,2048]{1,0:T(8,128)}, u32[]{:S(2)}) copy-start(f32[512,2048]{1,0:T(8,128)} %param.17) | copy-start | bytes 12582916
Sparse Core Ops, SparseCore 0:
  10.8 10.4 reduce-scatter.3
  24.1 8.8 reduce-scatter.5
  35.9 82.6 reduce-scatter.7
where the time goes:
time: 197 us; the launch traced here: 196 us
  waiting for transfers between devices  101 us (51%)
  blocking collectives  57.2 us (29%)
  between operations  15.9 us (8%)
  matrix products  13.3 us (7%)
  local copies, waits for them, and re-layouts  4.6 us (2%)
  other arithmetic  3.53 us (2%)
    reduce_scatter x1, waiting for transfers between devices, shards(): lax.psum_scatter(lax.dot_general(normed_input, joined, (((0,), (0,)), (()...  81.1 us
    psum x1, blocking collectives, shards(): total = lax.psum(local_total, ('fs', 'rep', 'tp'))  36.8 us
    reduce_scatter x1, waiting for transfers between devices, shards(): lax.psum_scatter(value_proj, 'tp', scatter_dimension=1, tiled=True)  10.8 us
    all_gather x1, blocking collectives, shards(): lax.all_gather(key_dir, 'rep', axis=0, tiled=True)  9.4 us
    reduce_scatter x1, waiting for transfers between devices, shards(): lax.psum_scatter(key_proj, 'tp', scatter_dimension=1, tiled=True)  9.18 us
    all_gather x1, blocking collectives, shards(): lax.all_gather(value_dir, 'rep', axis=0, tiled=True)  7.04 us
    unnamed x24, local copies, waits for them, and re-layouts  4.6 us
  transfers between devices with their start and end apart: 3, of which 3 were waited for; matrix products, arithmetic and copies ran while one was open for 3% of the time, Pallas kernels for 0%

commit v1 on v0

v1 whole, which is shorter than its diff:
```python
import functools

import jax
import jax.numpy as jnp
from jax import lax
from jax.experimental import pallas as pl
from jax.experimental.pallas import tpu as pltpu
from jax.sharding import PartitionSpec as P

first_decay = 0.8
second_decay = 0.9
root_epsilon = 1e-08
mean_epsilon = 1e-06
learn_rate = 0.01

F32 = jnp.float32
BF16 = jnp.bfloat16
MESH = pl.DeviceIdType.MESH


def moments(grad, moment, second):
    mean = first_decay * moment + (1.0 - first_decay) * grad
    square = second_decay * second + (1.0 - second_decay) * grad * grad
    return mean, square


def remote(src, dst, send, recv, where):
    return pltpu.make_async_remote_copy(
        src_ref=src, dst_ref=dst, send_sem=send, recv_sem=recv,
        device_id=where, device_id_type=MESH,
    )


def exchange(
    F, R,
    x, kc, vc, kb, vb, km, ks, vm, vs,
    gath, total, grad,
    x_v, kc_v, vc_v, kb_v, vb_v, km_v, ks_v, vm_v, vs_v,
    proj, proj_in, part, land1, out2, land2, sq1, sq2,
    load, p_send, p_recv, s1, r1, s2, r2, gs, gr, fs_, fr, q1s, q1r, q2s, q2r,
):
    f0, r0, t0 = lax.axis_index("fs"), lax.axis_index("rep"), lax.axis_index("tp")
    t1 = 1 - t0
    D = x.shape[1]
    rows, width = km.shape
    wire = part.dtype

    pairs = [(kc, kc_v), (kb, kb_v), (vc, vc_v), (vb, vb_v), (x, x_v),
             (km, km_v), (ks, ks_v), (vm, vm_v), (vs, vs_v)]
    loads = [pltpu.make_async_copy(a, b, load.at[i]) for i, (a, b) in enumerate(pairs)]
    for c in loads:
        c.start()

    barrier = pltpu.get_barrier_semaphore()

    def greet_fs(d, _):
        pl.semaphore_signal(barrier, inc=1, device_id={"fs": lax.rem(f0 + d, F)}, device_id_type=MESH)
        return 0

    lax.fori_loop(1, F, greet_fs, 0)
    group = [(k, t) for k in range(R) for t in range(2) if (k, t) != (0, 0)]
    for k, t in group:
        pl.semaphore_signal(
            barrier, inc=1,
            device_id={"rep": lax.rem(r0 + k, R), "tp": lax.rem(t0 + t, 2)},
            device_id_type=MESH,
        )

    for c in loads[:2]:
        c.wait()
    pk = jnp.dot(kc_v[...], kb_v[...], preferred_element_type=F32)
    for t in range(2):
        proj[t, :, :width] = pk[:, t * width:(t + 1) * width]
    for c in loads[2:4]:
        c.wait()
    pv = jnp.dot(vc_v[...], vb_v[...], preferred_element_type=F32)
    for t in range(2):
        proj[t, :, width:] = pv[:, t * width:(t + 1) * width]

    pl.semaphore_wait(barrier, F - 1 + 2 * R - 1)
    swap = remote(proj.at[t1], proj_in, p_send, p_recv, {"tp": t1})
    swap.start()
    loads[4].wait()
    swap.wait_recv()
    joined = (proj[t0] + proj_in[...]).astype(BF16)

    tile = min(256, D)
    for i in range(D // tile):
        g = lax.dot_general(
            x_v[:, i * tile:(i + 1) * tile], joined, (((0,), (0,)), ((), ())),
            preferred_element_type=F32,
        )
        for c in range(tile // rows):
            at = i * (tile // rows) + c
            part[at // R, at % R] = g[c * rows:(c + 1) * rows].astype(wire)

    def copy1(f, k):
        r = lax.rem(r0 + k, R)
        return remote(part.at[f, r], land1.at[f, r0], s1.at[f, r], r1.at[f, r0], {"rep": r})

    def wait1(f, k):
        r = lax.rem(r0 + k, R)
        remote(part.at[f, r], land1.at[f, r], s1.at[f, r], r1.at[f, r], {"rep": r}).wait_recv()

    def send1(d, _):
        f = lax.rem(f0 + d, F)
        for k in range(1, R):
            copy1(f, k).start()
        return 0

    lax.fori_loop(1, F + 1, send1, 0)

    def gather1(f):
        acc = part[f, r0].astype(F32)
        for k in range(1, R):
            wait1(f, k)
            acc = acc + land1[f, lax.rem(r0 + k, R)].astype(F32)
        return acc

    def send2(d, _):
        f = lax.rem(f0 + d, F)
        out2[f] = gather1(f).astype(wire)
        remote(out2.at[f], land2.at[f0], s2.at[f], r2.at[f0], {"fs": f}).start()
        return 0

    lax.fori_loop(1, F, send2, 0)
    for c in loads[5:]:
        c.wait()
    grad[...] = gather1(f0)

    def add2(d, _):
        f = lax.rem(f0 + d, F)
        remote(out2.at[f], land2.at[f], s2.at[f], r2.at[f], {"fs": f}).wait_recv()
        grad[...] += land2[f].astype(F32)
        return 0

    lax.fori_loop(1, F, add2, 0)

    squares = 0.0
    for h, (m_v, s_v) in enumerate(((km_v, ks_v), (vm_v, vs_v))):
        mean, square = moments(grad[:, h * width:(h + 1) * width], m_v[...], s_v[...])
        ratio = mean / (jnp.sqrt(square) + root_epsilon)
        gath[t0, r0, :, h * width:(h + 1) * width] = ratio.astype(BF16)
        squares = squares + jnp.sum(ratio * ratio, axis=0, keepdims=True)
    sq1[f0] = squares

    def sq1_copy(d):
        f = lax.rem(f0 + d, F)
        return remote(sq1.at[f0], sq1.at[f0], q1s.at[f], q1r.at[f0], {"fs": f})

    def sq1_wait(d, acc):
        f = lax.rem(f0 + d, F)
        remote(sq1.at[f], sq1.at[f], q1s.at[f], q1r.at[f], {"fs": f}).wait_recv()
        return acc

    def sq1_start(d, _):
        sq1_copy(d).start()
        return 0

    lax.fori_loop(1, F, sq1_start, 0)

    for k in range(1, R):
        r = lax.rem(r0 + k, R)
        remote(gath.at[t0, r0], gath.at[t0, r0], gs.at[r], gr.at[r0], {"rep": r}).start()

    def forward(r):
        return remote(gath.at[t0, r], gath.at[t0, r], fs_.at[r], fr.at[r], {"tp": t1})

    def forwarded(r):
        return remote(gath.at[t1, r], gath.at[t1, r], fs_.at[r], fr.at[r], {"tp": t1})

    forward(r0).start()

    lax.fori_loop(1, F, sq1_wait, 0)
    acc = sq1[0]
    for f in range(1, F):
        acc = acc + sq1[f]
    slot = t0 * R + r0
    sq2[slot] = acc

    def sq2_copy(k, t, which):
        r, tp = lax.rem(r0 + k, R), lax.rem(t0 + t, 2)
        other = tp * R + r
        here = slot if which == 0 else other
        return remote(sq2.at[here], sq2.at[here], q2s.at[other], q2r.at[here], {"rep": r, "tp": tp})

    for k, t in group:
        sq2_copy(k, t, 0).start()

    for k in range(1, R):
        r = lax.rem(r0 + k, R)
        remote(gath.at[t0, r], gath.at[t0, r], gs.at[r], gr.at[r], {"rep": r}).wait_recv()
        forward(r).start()

    for k, t in group:
        sq2_copy(k, t, 1).wait_recv()
    acc = sq2[0]
    for i in range(1, 2 * R):
        acc = acc + sq2[i]
    total[...] = acc

    for k in range(R):
        forwarded(lax.rem(r0 + k, R)).wait_recv()

    swap.wait_send()

    def drain1(d, _):
        f = lax.rem(f0 + d, F)
        for k in range(1, R):
            copy1(f, k).wait_send()
        return 0

    lax.fori_loop(1, F + 1, drain1, 0)

    def drain2(d, _):
        f = lax.rem(f0 + d, F)
        remote(out2.at[f], land2.at[f0], s2.at[f], r2.at[f0], {"fs": f}).wait_send()
        sq1_copy(d).wait_send()
        return 0

    lax.fori_loop(1, F, drain2, 0)
    for k in range(1, R):
        r = lax.rem(r0 + k, R)
        remote(gath.at[t0, r0], gath.at[t0, r0], gs.at[r], gr.at[r0], {"rep": r}).wait_send()
    for k in range(R):
        forward(lax.rem(r0 + k, R)).wait_send()
    for k, t in group:
        sq2_copy(k, t, 0).wait_send()


def finish(
    count, R,
    gath, total, grad, kb, vb, kmast, vmast, km, ks, vm, vs,
    kmean, ksquare, vmean, vsquare, kstep, vstep, kweight, vweight,
):
    width = km.shape[1]

    @pl.when(pl.program_id(0) == 0)
    def _():
        kmean[...], ksquare[...] = moments(grad[:, :width], km[...], ks[...])
        vmean[...], vsquare[...] = moments(grad[:, width:], vm[...], vs[...])

    whole = jnp.sum(total[...], axis=1, keepdims=True)
    inverse = 1.0 / jnp.sqrt(whole / count + mean_epsilon)
    for h, (basis, master, step, weight) in enumerate(
        ((kb, kmast, kstep, kweight), (vb, vmast, vstep, vweight))
    ):
        rows = jnp.concatenate(
            [gath[t, 0, :, h * width:(h + 1) * width] for t in range(2)], axis=1
        )
        out = lax.dot_general(
            rows, basis[...], (((1,), (1,)), ((), ())), preferred_element_type=F32
        ) * inverse
        step[...] = out
        weight[...] = (master[...] - learn_rate * out).astype(BF16)


def shards(F, R, x, kc, vc, kb, vb, kmast, vmast, km, ks, vm, vs):
    rows, width = km.shape
    both = 2 * width
    tok, D = x.shape
    wire = BF16 if rows % 16 == 0 else F32
    any_ = pl.BlockSpec(memory_space=pl.ANY)
    vmem = pl.BlockSpec(memory_space=pltpu.VMEM)
    dma = pltpu.SemaphoreType.DMA
    staged = (x, kc, vc, kb, vb, km, ks, vm, vs)
    gath, total, grad = pl.pallas_call(
        functools.partial(exchange, F, R),
        out_shape=(
            jax.ShapeDtypeStruct((2, R, rows, both), BF16),
            jax.ShapeDtypeStruct((1, width), F32),
            jax.ShapeDtypeStruct((rows, both), F32),
        ),
        in_specs=[any_] * 9,
        out_specs=(vmem,) * 3,
        scratch_shapes=[pltpu.VMEM(a.shape, a.dtype) for a in staged] + [
            pltpu.VMEM((2, tok, both), F32),
            pltpu.VMEM((tok, both), F32),
            pltpu.VMEM((F, R, rows, both), wire),
            pltpu.VMEM((F, R, rows, both), wire),
            pltpu.VMEM((F, rows, both), wire),
            pltpu.VMEM((F, rows, both), wire),
            pltpu.VMEM((F, 1, width), F32),
            pltpu.VMEM((2 * R, 1, width), F32),
            dma((9,)), dma, dma, dma((F, R)), dma((F, R)), dma((F,)), dma((F,)),
            dma((R,)), dma((R,)), dma((R,)), dma((R,)),
            dma((F,)), dma((F,)), dma((2 * R,)), dma((2 * R,)),
        ],
        compiler_params=pltpu.CompilerParams(collective_id=0, has_side_effects=True),
        name="exchange",
    )(x, kc, vc, kb, vb, km, ks, vm, vs)

    def row(a):
        return pl.BlockSpec((rows, a.shape[1]), lambda i: (i, 0))

    def fixed(a):
        return pl.BlockSpec(a.shape, lambda i: (0,) * len(a.shape))

    sds = jax.ShapeDtypeStruct
    return pl.pallas_call(
        functools.partial(finish, 2 * D * both, R),
        grid=(R,),
        out_shape=tuple(sds(a.shape, F32) for a in (km, ks, vm, vs, kmast, vmast))
        + tuple(sds(a.shape, BF16) for a in (kmast, vmast)),
        in_specs=[
            pl.BlockSpec((2, 1, rows, both), lambda i: (0, i, 0, 0)),
            fixed(total), fixed(grad), fixed(kb), fixed(vb), row(kmast), row(vmast),
            fixed(km), fixed(ks), fixed(vm), fixed(vs),
        ],
        out_specs=(fixed(km), fixed(ks), fixed(vm), fixed(vs),
                   row(kmast), row(vmast), row(kmast), row(vmast)),
        name="finish",
    )(gath, total, grad, kb, vb, kmast, vmast, km, ks, vm, vs)


def solution(mesh):
    rows = ("fs", "rep")
    placed = (
        (P(rows, None),) + (P(rows, "tp"),) * 2 + (P("tp", None),) * 2
        + (P("fs", "tp"),) * 2 + (P(rows, "tp"),) * 4
    )
    return jax.shard_map(
        functools.partial(shards, mesh.shape["fs"], mesh.shape["rep"]),
        mesh=mesh,
        in_specs=placed,
        out_specs=(P(rows, "tp"),) * 4 + (P("fs", "tp"),) * 4,
        check_vma=False,
    )
```

time: 197 us -> 40 us (0.20)
  waiting for transfers between devices: 101 us -> 0 us
  blocking collectives: 57.2 us -> 0 us
  Pallas kernels: 0 us -> 39.2 us
  between operations: 15.9 us -> 0.64 us
  matrix products: 13.3 us -> 0 us
  local copies, waits for them, and re-layouts: 4.6 us -> 0 us
  other arithmetic: 3.53 us -> 0 us
    reduce_scatter x3 -> x0, waiting for transfers between devices: 101 us -> none  [the longest x1 81.1 us: shards(): lax.psum_scatter(lax.dot_general(normed_input, joined, (((0,), (0,)), (()...]
    pallas_call x0 -> x2, Pallas kernels: none -> 39.2 us  [the longest x1 30.8 us: shards(): pl.pallas_call(functools.partial(exchange, F, R), out_shape=(jax.ShapeDty...]
    psum x1 -> x0, blocking collectives: 36.8 us -> none  [shards(): total = lax.psum(local_total, ('fs', 'rep', 'tp'))]
    all_gather x4 -> x0, blocking collectives: 20.4 us -> none  [the longest x1 9.4 us: shards(): lax.all_gather(key_dir, 'rep', axis=0, tiled=True)]
    dot_general x5 -> x0, matrix products: 13.3 us -> none  [the longest x1 3.48 us: shards(): lax.dot_general(value_dir, value_basis, dims, preferred_element_type=jnp....]
    unnamed x24 -> x0, local copies, waits for them, and re-layouts: 4.6 us -> none
  transfers between devices with their start and end apart: 3 -> 0, of which waited for: 3 -> 0; matrix products, arithmetic and copies ran while one was open for 3% -> 0% of each run, Pallas kernels for 0% -> 0%
where the time goes in v1:
time: 40 us; the launch traced here: 39.8 us
  Pallas kernels  39.2 us (98%)
  between operations  0.64 us (2%)
    pallas_call x1, Pallas kernels, shards(): pl.pallas_call(functools.partial(exchange, F, R), out_shape=(jax.ShapeDty...  30.8 us
    pallas_call x1, Pallas kernels, shards(): pl.pallas_call(functools.partial(finish, 2 * D * both, R), grid=(R,), out...  8.35 us

profile of v1, /device:TPU:0, one launch (start us, length us, event | category | flops | bytes accessed | tf_op | source)
XLA Modules:
  0.0 39.8 jit_solution(3790865093254210148)
XLA Ops:
  0.6 30.8 %exchange.1 = (bf16[2,4,128,256]{3,2,1,0:T(8,128)(2,1)}, f32[1,128]{1,0:T(1,128)}, f32[128,256]{1,0:T(8,128)}) custom-call(bf16[256,2048]{1,0:T(8,128)(2,1)} %x.1, bf16[256,1024]{1,0:T(8,128)(2,1)} %kc.1, bf16[256,2048]{1,0:T(8,128)(2,1)} %vc.1, bf16[1024,256]{1,0:T(8,128)(2,1)} %kb.3, bf16[2048,256]{1,0:T(8,128)(2,1)} %vb.3, f32[128,128]{1,0:T(8,128)} %km.3, ...), custom_call_target="tpu_custom_call" | custom-call | tf_op jit(solution)/shard_map/exchange/pallas_call | solution.py:267
  31.5 8.3 %finish.1 = (f32[128,128]{1,0:T(8,128)}, f32[128,128]{1,0:T(8,128)}, f32[128,128]{1,0:T(8,128)}, f32[128,128]{1,0:T(8,128)}, f32[512,1024]{1,0:T(8,128)}, /*inde...) custom-call(bf16[2,4,128,256]{3,2,1,0:T(8,128)(2,1)} %get-tuple-element.11.gath, ...), custom_call_target="tpu_custom_call" | custom-call | tf_op jit(solution)/shard_map/finish/pallas_call | solution.py:300

commit v2 on v1

--- a/solution.py
+++ b/solution.py
@@ -33,23 +33,16 @@
 
 def exchange(
     F, R,
-    x, kc, vc, kb, vb, km, ks, vm, vs,
+    x_v, kc_v, vc_v, kb_v, vb_v, km_v, ks_v, vm_v, vs_v,
     gath, total, grad,
-    x_v, kc_v, vc_v, kb_v, vb_v, km_v, ks_v, vm_v, vs_v,
     proj, proj_in, part, land1, out2, land2, sq1, sq2,
-    load, p_send, p_recv, s1, r1, s2, r2, gs, gr, fs_, fr, q1s, q1r, q2s, q2r,
+    p_send, p_recv, s1, r1, s2, r2, gs, gr, fs_, fr, q1s, q1r, q2s, q2r,
 ):
     f0, r0, t0 = lax.axis_index("fs"), lax.axis_index("rep"), lax.axis_index("tp")
     t1 = 1 - t0
-    D = x.shape[1]
-    rows, width = km.shape
+    D = x_v.shape[1]
+    rows, width = km_v.shape
     wire = part.dtype
-
-    pairs = [(kc, kc_v), (kb, kb_v), (vc, vc_v), (vb, vb_v), (x, x_v),
-             (km, km_v), (ks, ks_v), (vm, vm_v), (vs, vs_v)]
-    loads = [pltpu.make_async_copy(a, b, load.at[i]) for i, (a, b) in enumerate(pairs)]
-    for c in loads:
-        c.start()
 
     barrier = pltpu.get_barrier_semaphore()
 
@@ -66,13 +59,9 @@
             device_id_type=MESH,
         )
 
-    for c in loads[:2]:
-        c.wait()
     pk = jnp.dot(kc_v[...], kb_v[...], preferred_element_type=F32)
     for t in range(2):
         proj[t, :, :width] = pk[:, t * width:(t + 1) * width]
-    for c in loads[2:4]:
-        c.wait()
     pv = jnp.dot(vc_v[...], vb_v[...], preferred_element_type=F32)
     for t in range(2):
         proj[t, :, width:] = pv[:, t * width:(t + 1) * width]
@@ -80,7 +69,6 @@
     pl.semaphore_wait(barrier, F - 1 + 2 * R - 1)
     swap = remote(proj.at[t1], proj_in, p_send, p_recv, {"tp": t1})
     swap.start()
-    loads[4].wait()
     swap.wait_recv()
     joined = (proj[t0] + proj_in[...]).astype(BF16)
 
@@ -124,8 +112,6 @@
         return 0
 
     lax.fori_loop(1, F, send2, 0)
-    for c in loads[5:]:
-        c.wait()
     grad[...] = gather1(f0)
 
     def add2(d, _):
@@ -260,10 +246,8 @@
     both = 2 * width
     tok, D = x.shape
     wire = BF16 if rows % 16 == 0 else F32
-    any_ = pl.BlockSpec(memory_space=pl.ANY)
     vmem = pl.BlockSpec(memory_space=pltpu.VMEM)
     dma = pltpu.SemaphoreType.DMA
-    staged = (x, kc, vc, kb, vb, km, ks, vm, vs)
     gath, total, grad = pl.pallas_call(
         functools.partial(exchange, F, R),
         out_shape=(
@@ -271,9 +255,9 @@
             jax.ShapeDtypeStruct((1, width), F32),
             jax.ShapeDtypeStruct((rows, both), F32),
         ),
-        in_specs=[any_] * 9,
+        in_specs=[vmem] * 9,
         out_specs=(vmem,) * 3,
-        scratch_shapes=[pltpu.VMEM(a.shape, a.dtype) for a in staged] + [
+        scratch_shapes=[
             pltpu.VMEM((2, tok, both), F32),
             pltpu.VMEM((tok, both), F32),
             pltpu.VMEM((F, R, rows, both), wire),
@@ -282,11 +266,16 @@
             pltpu.VMEM((F, rows, both), wire),
             pltpu.VMEM((F, 1, width), F32),
             pltpu.VMEM((2 * R, 1, width), F32),
-            dma((9,)), dma, dma, dma((F, R)), dma((F, R)), dma((F,)), dma((F,)),
+            dma, dma, dma((F, R)), dma((F, R)), dma((F,)), dma((F,)),
             dma((R,)), dma((R,)), dma((R,)), dma((R,)),
             dma((F,)), dma((F,)), dma((2 * R,)), dma((2 * R,)),
         ],
-        compiler_params=pltpu.CompilerParams(collective_id=0, has_side_effects=True),
+        compiler_params=pltpu.CompilerParams(
+            collective_id=0, has_side_effects=True, vmem_limit_bytes=14 << 20
+        ),
+        cost_estimate=pl.CostEstimate(
+            flops=4 * tok * D * both, bytes_accessed=200 * x.size, transcendentals=0
+        ),
         name="exchange",
     )(x, kc, vc, kb, vb, km, ks, vm, vs)
 
@@ -298,7 +287,7 @@
 
     sds = jax.ShapeDtypeStruct
     return pl.pallas_call(
-        functools.partial(finish, 2 * D * both, R),
+        functools.partial(finish, 2 * D * kb.shape[1], R),
         grid=(R,),
         out_shape=tuple(sds(a.shape, F32) for a in (km, ks, vm, vs, kmast, vmast))
         + tuple(sds(a.shape, BF16) for a in (kmast, vmast)),
@@ -309,6 +298,11 @@
         ],
         out_specs=(fixed(km), fixed(ks), fixed(vm), fixed(vs),
                    row(kmast), row(vmast), row(kmast), row(vmast)),
+        compiler_params=pltpu.CompilerParams(vmem_limit_bytes=16 << 20),
+        cost_estimate=pl.CostEstimate(
+            flops=2 * R * rows * both * (kmast.shape[1] + vmast.shape[1]),
+            bytes_accessed=10 * (kmast.size + vmast.size), transcendentals=0,
+        ),
         name="finish",
     )(gath, total, grad, kb, vb, kmast, vmast, km, ks, vm, vs)
 

time: 40 us -> 47.1 us (1.18)
  local copies, waits for them, and re-layouts: 0 us -> 11.3 us
  Pallas kernels: 39.2 us -> 34.6 us
    unnamed x0 -> x24, local copies, waits for them, and re-layouts: none -> 11.3 us
    pallas_call x1, Pallas kernels: 8.35 us -> 4.72 us  [shards(): pl.pallas_call(functools.partial(finish, 2 * D * kb.shape[1], R), grid=(R...]
    pallas_call x1, Pallas kernels: 30.8 us -> 29.9 us  [shards(): pl.pallas_call(functools.partial(exchange, F, R), out_shape=(jax.ShapeDty...]
where the time goes in v2:
time: 47.1 us; the launch traced here: 46.6 us
  Pallas kernels  34.6 us (73%)
  local copies, waits for them, and re-layouts  11.3 us (24%)
  between operations  0.69 us (1%)
    pallas_call x1, Pallas kernels, shards(): pl.pallas_call(functools.partial(exchange, F, R), out_shape=(jax.ShapeDty...  29.9 us
    unnamed x24, local copies, waits for them, and re-layouts  11.3 us
    pallas_call x1, Pallas kernels, shards(): pl.pallas_call(functools.partial(finish, 2 * D * kb.shape[1], R), grid=(R...  4.72 us

profile of v2, /device:TPU:0, one launch (start us, length us, event | category | flops | bytes accessed | tf_op | source)
XLA Modules:
  0.0 46.6 jit_solution(2212305315017266702)
XLA Ops:
  0.6 0.0 copy-start
  0.6 1.2 %copy-done = bf16[2048,256]{1,0:T(8,128)(2,1)S(1)} copy-done((bf16[2048,256]{1,0:T(8,128)(2,1)S(1)}, bf16[2048,256]{1,0:T(8,128)(2,1)}, u32[]{:S(2)}) %copy-start) | copy-done | bytes 1048600
  1.9 0.0 copy-start.4
  1.9 1.0 %copy-done.4 = bf16[1024,256]{1,0:T(8,128)(2,1)S(1)} copy-done((bf16[1024,256]{1,0:T(8,128)(2,1)S(1)}, bf16[1024,256]{1,0:T(8,128)(2,1)}, u32[]{:S(2)}) %copy-start.4) | copy-done | bytes 524312
  2.9 0.0 copy-start.5
  2.9 1.2 %copy-done.5 = bf16[256,2048]{1,0:T(8,128)(2,1)S(1)} copy-done((bf16[256,2048]{1,0:T(8,128)(2,1)S(1)}, bf16[256,2048]{1,0:T(8,128)(2,1)}, u32[]{:S(2)}) %copy-start.5) | copy-done | bytes 1048600
  4.1 0.0 copy-start.6
  4.1 1.2 %copy-done.6 = bf16[256,2048]{1,0:T(8,128)(2,1)S(1)} copy-done((bf16[256,2048]{1,0:T(8,128)(2,1)S(1)}, bf16[256,2048]{1,0:T(8,128)(2,1)}, u32[]{:S(2)}) %copy-start.6) | copy-done | bytes 1048600
  5.4 0.0 copy-start.7
  5.4 1.0 %copy-done.7 = bf16[256,1024]{1,0:T(8,128)(2,1)S(1)} copy-done((bf16[256,1024]{1,0:T(8,128)(2,1)S(1)}, bf16[256,1024]{1,0:T(8,128)(2,1)}, u32[]{:S(2)}) %copy-start.7) | copy-done | bytes 524312
  6.4 0.0 copy-start.8
  6.4 0.8 %copy-done.8 = f32[128,128]{1,0:T(8,128)S(1)} copy-done((f32[128,128]{1,0:T(8,128)S(1)}, f32[128,128]{1,0:T(8,128)}, u32[]{:S(2)}) %copy-start.8) | copy-done | bytes 65560
  7.2 0.0 copy-start.9
  7.2 0.8 %copy-done.9 = f32[128,128]{1,0:T(8,128)S(1)} copy-done((f32[128,128]{1,0:T(8,128)S(1)}, f32[128,128]{1,0:T(8,128)}, u32[]{:S(2)}) %copy-start.9) | copy-done | bytes 65560
  8.1 0.0 copy-start.10
  8.1 0.8 %copy-done.10 = f32[128,128]{1,0:T(8,128)S(1)} copy-done((f32[128,128]{1,0:T(8,128)S(1)}, f32[128,128]{1,0:T(8,128)}, u32[]{:S(2)}) %copy-start.10) | copy-done | bytes 65560
  8.9 0.0 copy-start.11
  8.9 0.8 %copy-done.11 = f32[128,128]{1,0:T(8,128)S(1)} copy-done((f32[128,128]{1,0:T(8,128)S(1)}, f32[128,128]{1,0:T(8,128)}, u32[]{:S(2)}) %copy-start.11) | copy-done | bytes 65560
  9.8 0.0 copy-start.1
  9.8 0.0 copy-start.3
  9.8 29.9 %exchange.1 = (bf16[2,4,128,256]{3,2,1,0:T(8,128)(2,1)S(1)}, f32[1,128]{1,0:T(1,128)S(1)}, f32[128,256]{1,0:T(8,128)S(1)}) custom-call(bf16[256,2048]{1,0:T(8,128)(2,1)S(1)} %copy-done.5, bf16[256,1024]{1,0:T(8,128)(2,1)S(1)} %copy-done.7, bf16[256,2048]{1,0:T(8,128)(2,1)S(1)} %copy-done.6, bf16[1024,256]{1,0:T(8,128)(2,1)S(1)} %copy-done.4, ...), custom_call_target="tpu_custom_call" | custom-call | flops 536870912 | bytes 104857600 | tf_op jit(solution)/shard_map/exchange/pallas_call | solution.py:251
  39.7 0.0 copy-done.1
  39.7 0.0 copy-done.3
  39.7 0.0 copy-start.2
  39.7 2.2 %copy-done.2 = f32[512,2048]{1,0:T(8,128)S(1)} copy-done((f32[512,2048]{1,0:T(8,128)S(1)}, f32[512,2048]{1,0:T(8,128)}, u32[]{:S(2)}) %copy-start.2) | copy-done | bytes 4194328
  41.9 4.7 %finish.1 = (f32[128,128]{1,0:T(8,128)}, f32[128,128]{1,0:T(8,128)}, f32[128,128]{1,0:T(8,128)}, f32[128,128]{1,0:T(8,128)}, f32[512,1024]{1,0:T(8,128)}, /*inde...) custom-call(bf16[2,4,128,256]{3,2,1,0:T(8,128)(2,1)S(1)} %get-tuple-element.11.gath, ...), custom_call_target="tpu_custom_call" | custom-call | flops 805306368 | bytes 15728640 | tf_op jit(solution)/shard_map/finish/pallas_call | solution.py:289
Async XLA Ops:
  0.6 1.2 %copy-start = (bf16[2048,256]{1,0:T(8,128)(2,1)S(1)}, bf16[2048,256]{1,0:T(8,128)(2,1)}, u32[]{:S(2)}) copy-start(bf16[2048,256]{1,0:T(8,128)(2,1)} %vb.1) | copy-start | bytes 3145732
  1.9 1.0 %copy-start.4 = (bf16[1024,256]{1,0:T(8,128)(2,1)S(1)}, bf16[1024,256]{1,0:T(8,128)(2,1)}, u32[]{:S(2)}) copy-start(bf16[1024,256]{1,0:T(8,128)(2,1)} %kb.1) | copy-start | bytes 1572868
  2.9 1.2 %copy-start.5 = (bf16[256,2048]{1,0:T(8,128)(2,1)S(1)}, bf16[256,2048]{1,0:T(8,128)(2,1)}, u32[]{:S(2)}) copy-start(bf16[256,2048]{1,0:T(8,128)(2,1)} %x_v.1) | copy-start | bytes 3145732
  4.1 1.2 %copy-start.6 = (bf16[256,2048]{1,0:T(8,128)(2,1)S(1)}, bf16[256,2048]{1,0:T(8,128)(2,1)}, u32[]{:S(2)}) copy-start(bf16[256,2048]{1,0:T(8,128)(2,1)} %vc_v.1) | copy-start | bytes 3145732
  5.4 1.0 %copy-start.7 = (bf16[256,1024]{1,0:T(8,128)(2,1)S(1)}, bf16[256,1024]{1,0:T(8,128)(2,1)}, u32[]{:S(2)}) copy-start(bf16[256,1024]{1,0:T(8,128)(2,1)} %kc_v.1) | copy-start | bytes 1572868
  6.4 0.8 %copy-start.8 = (f32[128,128]{1,0:T(8,128)S(1)}, f32[128,128]{1,0:T(8,128)}, u32[]{:S(2)}) copy-start(f32[128,128]{1,0:T(8,128)} %km.1) | copy-start | bytes 196612
  7.2 0.8 %copy-start.9 = (f32[128,128]{1,0:T(8,128)S(1)}, f32[128,128]{1,0:T(8,128)}, u32[]{:S(2)}) copy-start(f32[128,128]{1,0:T(8,128)} %ks.1) | copy-start | bytes 196612
  8.1 0.8 %copy-start.10 = (f32[128,128]{1,0:T(8,128)S(1)}, f32[128,128]{1,0:T(8,128)}, u32[]{:S(2)}) copy-start(f32[128,128]{1,0:T(8,128)} %vm.1) | copy-start | bytes 196612
  8.9 0.8 %copy-start.11 = (f32[128,128]{1,0:T(8,128)S(1)}, f32[128,128]{1,0:T(8,128)}, u32[]{:S(2)}) copy-start(f32[128,128]{1,0:T(8,128)} %vs.1) | copy-start | bytes 196612
  9.8 29.9 %copy-start.1 = (bf16[2048,256]{1,0:T(8,128)(2,1)S(1)}, bf16[2048,256]{1,0:T(8,128)(2,1)}, u32[]{:S(2)}) copy-start(bf16[2048,256]{1,0:T(8,128)(2,1)} %vb.1) | copy-start | bytes 3145732
  9.8 29.9 %copy-start.3 = (f32[512,1024]{1,0:T(8,128)S(1)}, f32[512,1024]{1,0:T(8,128)}, u32[]{:S(2)}) copy-start(f32[512,1024]{1,0:T(8,128)} %kmast.1) | copy-start | bytes 6291460
  39.7 2.2 %copy-start.2 = (f32[512,2048]{1,0:T(8,128)S(1)}, f32[512,2048]{1,0:T(8,128)}, u32[]{:S(2)}) copy-start(f32[512,2048]{1,0:T(8,128)} %vmast.1) | copy-start | bytes 12582916

commit v3 on v1

--- a/solution.py
+++ b/solution.py
@@ -84,16 +84,6 @@
     swap.wait_recv()
     joined = (proj[t0] + proj_in[...]).astype(BF16)
 
-    tile = min(256, D)
-    for i in range(D // tile):
-        g = lax.dot_general(
-            x_v[:, i * tile:(i + 1) * tile], joined, (((0,), (0,)), ((), ())),
-            preferred_element_type=F32,
-        )
-        for c in range(tile // rows):
-            at = i * (tile // rows) + c
-            part[at // R, at % R] = g[c * rows:(c + 1) * rows].astype(wire)
-
     def copy1(f, k):
         r = lax.rem(r0 + k, R)
         return remote(part.at[f, r], land1.at[f, r0], s1.at[f, r], r1.at[f, r0], {"rep": r})
@@ -108,7 +98,32 @@
             copy1(f, k).start()
         return 0
 
-    lax.fori_loop(1, F + 1, send1, 0)
+    span = R * rows
+    if span % 256 == 0 and 256 % rows == 0:
+        def make_and_send(d, _):
+            f = lax.rem(f0 + d, F)
+            for i in range(span // 256):
+                at = pl.multiple_of(f * span + i * 256, 256)
+                g = lax.dot_general(
+                    x_v[:, pl.ds(at, 256)], joined, (((0,), (0,)), ((), ())),
+                    preferred_element_type=F32,
+                )
+                for c in range(256 // rows):
+                    part[f, i * (256 // rows) + c] = g[c * rows:(c + 1) * rows].astype(wire)
+            return send1(d, 0)
+
+        lax.fori_loop(1, F + 1, make_and_send, 0, unroll=True)
+    else:
+        tile = min(256, D)
+        for i in range(D // tile):
+            g = lax.dot_general(
+                x_v[:, i * tile:(i + 1) * tile], joined, (((0,), (0,)), ((), ())),
+                preferred_element_type=F32,
+            )
+            for c in range(tile // rows):
+                at = i * (tile // rows) + c
+                part[at // R, at % R] = g[c * rows:(c + 1) * rows].astype(wire)
+        lax.fori_loop(1, F + 1, send1, 0)
 
     def gather1(f):
         acc = part[f, r0].astype(F32)

time: 40 us -> 39.8 us (level)
  no operation moved by 1% of the time
where the time goes in v3:
time: 39.8 us; the launch traced here: 39.6 us
  Pallas kernels  38.9 us (98%)
  between operations  0.64 us (2%)
    pallas_call x1, Pallas kernels, shards(): pl.pallas_call(functools.partial(exchange, F, R), out_shape=(jax.ShapeDty...  30.6 us
    pallas_call x1, Pallas kernels, shards(): pl.pallas_call(functools.partial(finish, 2 * D * both, R), grid=(R,), out...  8.35 us

profile of v3, /device:TPU:0, one launch (start us, length us, event | category | flops | bytes accessed | tf_op | source)
XLA Modules:
  0.0 39.6 jit_solution(3935202712235541089)
XLA Ops:
  0.6 30.6 %exchange.1 = (bf16[2,4,128,256]{3,2,1,0:T(8,128)(2,1)}, f32[1,128]{1,0:T(1,128)}, f32[128,256]{1,0:T(8,128)}) custom-call(bf16[256,2048]{1,0:T(8,128)(2,1)} %x.1, bf16[256,1024]{1,0:T(8,128)(2,1)} %kc.1, bf16[256,2048]{1,0:T(8,128)(2,1)} %vc.1, bf16[1024,256]{1,0:T(8,128)(2,1)} %kb.3, bf16[2048,256]{1,0:T(8,128)(2,1)} %vb.3, f32[128,128]{1,0:T(8,128)} %km.3, ...), custom_call_target="tpu_custom_call" | custom-call | tf_op jit(solution)/shard_map/exchange/pallas_call | solution.py:282
  31.2 8.4 %finish.1 = (f32[128,128]{1,0:T(8,128)}, f32[128,128]{1,0:T(8,128)}, f32[128,128]{1,0:T(8,128)}, f32[128,128]{1,0:T(8,128)}, f32[512,1024]{1,0:T(8,128)}, /*inde...) custom-call(bf16[2,4,128,256]{3,2,1,0:T(8,128)(2,1)} %get-tuple-element.11.gath, ...), custom_call_target="tpu_custom_call" | custom-call | tf_op jit(solution)/shard_map/finish/pallas_call | solution.py:315
